TPU v7x, 32 devices: a whole 2x2x4 slice. The times are simulated.
32 devices in a mesh: rep: 2 (over x), fs: 4 (over y, core), tp: 4 (over z).
Axes of the slice: x: 2, y: 2, z: 4, core: 2. Of those that a mesh axis runs over, the one named last changes fastest.
Arguments:
- acts: bfloat16 [2048, 2048], P(('rep', 'fs'), 'tp'), may hold values from -6 to 6
- cotangent: bfloat16 [2048, 2048], P(('rep', 'fs'), 'tp'), may hold values from -8 to 8
- pre_act: bfloat16 [2048, 4096], P(('rep', 'fs'), 'tp'), may hold values from -6 to 6
- up_store: float32 [2048, 4096], P('fs', 'tp'), may hold values from -0.125 to 0.125
- up_scale: float32 [4096], P('tp'), may hold values from 0.5 to 2
- down_store: float32 [4096, 2048], P('tp', 'fs'), may hold values from -0.09375 to 0.09375
- down_scale: float32 [2048], replicated, may hold values from 0.5 to 2
Outputs:
- grad_input: bfloat16 [2048, 2048], P(('rep', 'fs'), 'tp')
- grad_up: float32 [2048, 4096], P('fs', 'tp')
- grad_down: float32 [4096, 2048], P('tp', 'fs')
All inputs are finite; a program needn't handle non-finite values.
Results may differ from a plain program's by a relative error of at most 0.007.
Values may be sent and summed in bfloat16 or wider, within the bound.
No kernel may reach another device: no remote copies, remote signals or barrier semaphores. Data moves between devices by JAX's collectives and lax.ppermute only.
A program may use at most 128 MiB of HBM per device.

v0:
```python
import math

import jax
import jax.numpy as jnp
from jax import lax
from jax.sharding import PartitionSpec as P


BOTH = ("fs", "tp")


def contract_last(left, right):
    return lax.dot_general(
        left, right, (((1,), (1,)), ((), ())), preferred_element_type=jnp.float32
    )


def contract_first(left, right):
    return lax.dot_general(
        left, right, (((0,), (0,)), ((), ())), preferred_element_type=jnp.float32
    )


def round_bf16(x):
    return lax.reduce_precision(x, exponent_bits=8, mantissa_bits=7)


def rep_sum(x):
    if lax.axis_size("rep") != 2:
        return lax.psum(x, "rep")
    own = round_bf16(x)
    other = lax.ppermute(own.astype(jnp.bfloat16), "rep", [(0, 1), (1, 0)])
    return own + other.astype(jnp.float32)


def body(acts, cotangent, pre_act, up_store, up_scale, down_store, down_scale):
    nf, nt = lax.axis_size("fs"), lax.axis_size("tp")
    per = nf // nt
    f, t = lax.axis_index("fs"), lax.axis_index("tp")
    tok, cols = acts.shape
    width = up_store.shape[0]
    norm_factor = 1.0 / math.sqrt(tok * nf * lax.axis_size("rep"))
    slots = [(s, a) for s in range(nt) for a in range(per)]

    def token_block(fi, ti, s, a):
        return (fi + (ti - s) * per + a) % nf

    def grid(target):
        return [
            (fi * nt + ti, target(fi, ti)) for fi in range(nf) for ti in range(nt)
        ]

    def to_owner(s, a):
        return grid(lambda fi, ti: token_block(fi, ti, s, a) * nt + ti)

    def from_owner(s, a):
        return [(dst, src) for src, dst in to_owner(s, a)]

    def home(a):
        return grid(lambda fi, ti: token_block(fi, ti, 0, a) * nt + fi // per)

    def away(a):
        return [(dst, src) for src, dst in home(a)]

    def part_at(a):
        return ((f - a) % per) * width

    def to_features(x):
        base = []
        for a in range(per):
            piece = x if per == 1 else lax.dynamic_slice_in_dim(x, part_at(a), width, 1)
            base.append(lax.ppermute(piece, BOTH, away(a)))
        return [
            base[a]
            if s == 0
            else lax.ppermute(base[a], "tp", [(i, (i + s) % nt) for i in range(nt)])
            for s, a in slots
        ]

    scale_here = lax.dynamic_slice_in_dim(down_scale, t * cols, cols, 0)
    scaled = (cotangent.astype(jnp.float32) * scale_here[None, :]).astype(jnp.bfloat16)
    scaled_blocks = to_features(scaled)
    positive = jnp.maximum(pre_act.astype(jnp.float32), 0.0)
    act = (positive * positive).astype(jnp.bfloat16)
    down_bf = down_store.astype(jnp.bfloat16)
    up_bf = up_store.astype(jnp.bfloat16)

    d_act = 0.0
    for (s, a), block in zip(slots, scaled_blocks):
        partial_value = contract_last(block, down_bf).astype(jnp.bfloat16)
        d_act += lax.ppermute(partial_value, BOTH, to_owner(s, a)).astype(jnp.float32)
    late_pre, d_act = lax.optimization_barrier((pre_act, d_act))
    positive = jnp.maximum(late_pre.astype(jnp.float32), 0.0)
    d_pre = (2.0 * positive * d_act * up_scale[None, :]).astype(jnp.bfloat16)

    act_blocks = [lax.ppermute(act, BOTH, from_owner(s, a)) for s, a in slots]
    acts_blocks = to_features(acts)
    grad_down = rep_sum(
        contract_first(jnp.concatenate(act_blocks), jnp.concatenate(scaled_blocks)) * norm_factor
    )

    dpre_blocks = [lax.ppermute(d_pre, BOTH, from_owner(s, a)) for s, a in slots]
    sums = [0.0] * per
    for (s, a), block in zip(slots, dpre_blocks):
        value = contract_last(block, up_bf)
        if s:
            value = lax.ppermute(
                value.astype(jnp.bfloat16), "tp", [(i, (i - s) % nt) for i in range(nt)]
            ).astype(jnp.float32)
        sums[a] += value
    pieces = [lax.ppermute(sums[a].astype(jnp.bfloat16), BOTH, home(a)) for a in range(per)]
    if per == 1:
        grad_input = pieces[0]
    else:
        grad_input = jnp.zeros((tok, cols), jnp.bfloat16)
        for a in range(per):
            grad_input = lax.dynamic_update_slice_in_dim(grad_input, pieces[a], part_at(a), 1)

    grad_up = rep_sum(
        contract_first(jnp.concatenate(acts_blocks), jnp.concatenate(dpre_blocks)) * norm_factor
    )
    return (grad_input, grad_up, grad_down)


def solution(mesh):
    return jax.shard_map(
        body,
        mesh=mesh,
        in_specs=(
            P(("rep", "fs"), "tp"),
            P(("rep", "fs"), "tp"),
            P(("rep", "fs"), "tp"),
            P("fs", "tp"),
            P("tp"),
            P("tp", "fs"),
            P(),
        ),
        out_specs=(P(("rep", "fs"), "tp"), P("fs", "tp"), P("tp", "fs")),
        check_vma=False,
    )
```

profile of v0, /device:TPU:0, one launch (start us, length us, event | category | flops | bytes accessed | tf_op | source)
XLA Modules:
  0.0 151.9 jit_solution(7853239412610663304)
XLA Ops:
  0.6 0.8 dynamic_slice.3
  1.4 1.0 multiply_convert_fusion.2
  2.4 0.7 collective-permute-start
  3.1 1.7 %convert_element_type.83 = bf16[1024,512]{1,0:T(8,128)(2,1)S(1)} convert(f32[1024,512]{1,0:T(8,128)} %param.12) | non-fusion elementwise | flops 524288 | bytes 3145728 | tf_op jit(solution)/shard_map/convert_element_type | solution.py:85
  4.8 15.5 %collective-permute-start.6 = (bf16[256,512]{1,0:T(8,128)(2,1)S(1)}, bf16[256,512]{1,0:T(8,128)(2,1)S(1)}, u32[]{:S(2)}, u32[]{:S(2)}) collective-permute-start(bf16[256,512]{1,0:T(8,128)(2,1)S(1)} %collective-permute-done), channel_id=1, source_target_pairs={{0,3},{1,0},{2,1},{3,2},{4,7},{5,4},{6,5},{7,6},{8,11},{9,8},{10,9... | collective-permute-start | bytes 786440 | tf_op jit(solution)/shard_map/ppermute | solution.py:76
  20.3 0.5 convolution_convert_fusion.3
  20.8 0.7 collective-permute-start.1
  21.5 2.3 %collective-permute-start.4 = (bf16[256,512]{1,0:T(8,128)(2,1)S(1)}, bf16[256,512]{1,0:T(8,128)(2,1)S(1)}, u32[]{:S(2)}, u32[]{:S(2)}) collective-permute-start(bf16[256,512]{1,0:T(8,128)(2,1)S(1)} %collective-permute-done), channel_id=1, source_target_pairs={{0,2},{1,3},{2,0},{3,1},{4,6},{5,7},{6,4},{7,5},{8,10},{9,11},{10,... | collective-permute-start | bytes 786440 | tf_op jit(solution)/shard_map/ppermute | solution.py:76
  23.8 0.4 collective-permute-done.6
  24.2 0.5 convolution_convert_fusion
  24.7 4.2 %collective-permute-start.7 = (bf16[256,1024]{1,0:T(8,128)(2,1)S(1)}, bf16[256,1024]{1,0:T(8,128)(2,1)S(1)}, u32[]{:S(2)}, u32[]{:S(2)}) collective-permute-start(bf16[256,1024]{1,0:T(8,128)(2,1)S(1)} %convolution_convert_fusion), channel_id=1, source_target_pairs={{0,4},{1,9},{2,14},{3,3},{4,8},{5,13},{6,2},{7,7},{8,12},{9,1},{10... | collective-permute-start | bytes 1572872 | tf_op jit(solution)/shard_map/ppermute | solution.py:91
  28.9 13.3 %collective-permute-done.4 = bf16[256,512]{1,0:T(8,128)(2,1)S(1)} collective-permute-done((bf16[256,512]{1,0:T(8,128)(2,1)S(1)}, bf16[256,512]{1,0:T(8,128)(2,1)S(1)}, u32[]{:S(2)}, u32[]{:S(2)}) %collective-permute-start.4) | collective-permute-done | bytes 262176 | tf_op jit(solution)/shard_map/ppermute | solution.py:76
  42.3 0.5 convolution_convert_fusion.1
  42.8 2.9 %collective-permute-start.5 = (bf16[256,1024]{1,0:T(8,128)(2,1)S(1)}, bf16[256,1024]{1,0:T(8,128)(2,1)S(1)}, u32[]{:S(2)}, u32[]{:S(2)}) collective-permute-start(bf16[256,1024]{1,0:T(8,128)(2,1)S(1)} %convolution_convert_fusion.1), channel_id=1, source_target_pairs={{0,8},{1,13},{2,2},{3,7},{4,12},{5,1},{6,6},{7,11},{8,0},{9,5},{10... | collective-permute-start | bytes 1572872 | tf_op jit(solution)/shard_map/ppermute | solution.py:91
  45.7 0.5 convolution_convert_fusion.2
  46.2 3.0 %collective-permute-start.3 = (bf16[256,1024]{1,0:T(8,128)(2,1)S(1)}, bf16[256,1024]{1,0:T(8,128)(2,1)S(1)}, u32[]{:S(2)}, u32[]{:S(2)}) collective-permute-start(bf16[256,1024]{1,0:T(8,128)(2,1)S(1)} %convolution_convert_fusion.2), channel_id=1, source_target_pairs={{0,12},{1,1},{2,6},{3,11},{4,0},{5,5},{6,10},{7,15},{8,4},{9,9},{1... | collective-permute-start | bytes 1572872 | tf_op jit(solution)/shard_map/ppermute | solution.py:91
  49.4 2.1 %collective-permute-start.24 = (bf16[256,1024]{1,0:T(8,128)(2,1)S(1)}, bf16[256,1024]{1,0:T(8,128)(2,1)S(1)}, u32[]{:S(2)}, u32[]{:S(2)}) collective-permute-start(bf16[256,1024]{1,0:T(8,128)(2,1)S(1)} %multiply_convert_fusion), channel_id=1, source_target_pairs={{4,0},{9,1},{14,2},{3,3},{8,4},{13,5},{2,6},{7,7},{12,8},{1,9},{6,... | collective-permute-start | bytes 1572872 | tf_op jit(solution)/shard_map/ppermute | solution.py:96
  51.5 2.9 %collective-permute-start.23 = (bf16[256,1024]{1,0:T(8,128)(2,1)S(1)}, bf16[256,1024]{1,0:T(8,128)(2,1)S(1)}, u32[]{:S(2)}, u32[]{:S(2)}) collective-permute-start(bf16[256,1024]{1,0:T(8,128)(2,1)S(1)} %multiply_convert_fusion), channel_id=1, source_target_pairs={{8,0},{13,1},{2,2},{7,3},{12,4},{1,5},{6,6},{11,7},{0,8},{5,9},{10... | collective-permute-start | bytes 1572872 | tf_op jit(solution)/shard_map/ppermute | solution.py:96
  54.4 1.9 %collective-permute-start.22 = (bf16[256,1024]{1,0:T(8,128)(2,1)S(1)}, bf16[256,1024]{1,0:T(8,128)(2,1)S(1)}, u32[]{:S(2)}, u32[]{:S(2)}) collective-permute-start(bf16[256,1024]{1,0:T(8,128)(2,1)S(1)} %multiply_convert_fusion), channel_id=1, source_target_pairs={{12,0},{1,1},{6,2},{11,3},{0,4},{5,5},{10,6},{15,7},{4,8},{9,9},{1... | collective-permute-start | bytes 1572872 | tf_op jit(solution)/shard_map/ppermute | solution.py:96
  56.3 3.1 %collective-permute-done.5 = bf16[256,1024]{1,0:T(8,128)(2,1)S(1)} collective-permute-done((bf16[256,1024]{1,0:T(8,128)(2,1)S(1)}, bf16[256,1024]{1,0:T(8,128)(2,1)S(1)}, u32[]{:S(2)}, u32[]{:S(2)}) %collective-permute-start.5) | collective-permute-done | bytes 524320 | tf_op jit(solution)/shard_map/ppermute | solution.py:91
  59.5 0.7 collective-permute-start.21
  60.1 9.1 %collective-permute-done.3 = bf16[256,1024]{1,0:T(8,128)(2,1)S(1)} collective-permute-done((bf16[256,1024]{1,0:T(8,128)(2,1)S(1)}, bf16[256,1024]{1,0:T(8,128)(2,1)S(1)}, u32[]{:S(2)}, u32[]{:S(2)}) %collective-permute-start.3) | collective-permute-done | bytes 524320 | tf_op jit(solution)/shard_map/ppermute | solution.py:91
  69.2 0.7 collective-permute-start.16
  70.5 11.9 %collective-permute-start.13 = (bf16[256,1024]{1,0:T(8,128)(2,1)S(1)}, bf16[256,1024]{1,0:T(8,128)(2,1)S(1)}, u32[]{:S(2)}, u32[]{:S(2)}) collective-permute-start(bf16[256,1024]{1,0:T(8,128)(2,1)S(1)} %multiply_convert_fusion.1), channel_id=1, source_target_pairs={{4,0},{9,1},{14,2},{3,3},{8,4},{13,5},{2,6},{7,7},{12,8},{1,9},{6,... | collective-permute-start | bytes 1572872 | tf_op jit(solution)/shard_map/ppermute | solution.py:102
  82.5 1.0 collective-permute-start.19
  83.6 3.8 %collective-permute-done.23 = bf16[256,1024]{1,0:T(8,128)(2,1)S(1)} collective-permute-done((bf16[256,1024]{1,0:T(8,128)(2,1)S(1)}, bf16[256,1024]{1,0:T(8,128)(2,1)S(1)}, u32[]{:S(2)}, u32[]{:S(2)}) %collective-permute-start.23) | collective-permute-done | bytes 524320 | tf_op jit(solution)/shard_map/ppermute | solution.py:96
  87.4 2.3 %collective-permute-start.11 = (bf16[256,1024]{1,0:T(8,128)(2,1)S(1)}, bf16[256,1024]{1,0:T(8,128)(2,1)S(1)}, u32[]{:S(2)}, u32[]{:S(2)}) collective-permute-start(bf16[256,1024]{1,0:T(8,128)(2,1)S(1)} %multiply_convert_fusion.1), channel_id=1, source_target_pairs={{8,0},{13,1},{2,2},{7,3},{12,4},{1,5},{6,6},{11,7},{0,8},{5,9},{10... | collective-permute-start | bytes 1572872 | tf_op jit(solution)/shard_map/ppermute | solution.py:102
  89.6 1.3 fusion.17
  90.9 0.7 collective-permute-start.8
  91.7 2.2 %collective-permute-done.13 = bf16[256,1024]{1,0:T(8,128)(2,1)S(1)} collective-permute-done((bf16[256,1024]{1,0:T(8,128)(2,1)S(1)}, bf16[256,1024]{1,0:T(8,128)(2,1)S(1)}, u32[]{:S(2)}, u32[]{:S(2)}) %collective-permute-start.13) | collective-permute-done | bytes 524320 | tf_op jit(solution)/shard_map/ppermute | solution.py:102
  93.8 4.1 %collective-permute-start.9 = (bf16[256,1024]{1,0:T(8,128)(2,1)S(1)}, bf16[256,1024]{1,0:T(8,128)(2,1)S(1)}, u32[]{:S(2)}, u32[]{:S(2)}) collective-permute-start(bf16[256,1024]{1,0:T(8,128)(2,1)S(1)} %multiply_convert_fusion.1), channel_id=1, source_target_pairs={{12,0},{1,1},{6,2},{11,3},{0,4},{5,5},{10,6},{15,7},{4,8},{9,9},{1... | collective-permute-start | bytes 1572872 | tf_op jit(solution)/shard_map/ppermute | solution.py:102
  97.9 0.5 convolution_convert_fusion.4
  98.4 8.7 %collective-permute-done.11 = bf16[256,1024]{1,0:T(8,128)(2,1)S(1)} collective-permute-done((bf16[256,1024]{1,0:T(8,128)(2,1)S(1)}, bf16[256,1024]{1,0:T(8,128)(2,1)S(1)}, u32[]{:S(2)}, u32[]{:S(2)}) %collective-permute-start.11) | collective-permute-done | bytes 524320 | tf_op jit(solution)/shard_map/ppermute | solution.py:102
  107.1 0.5 convolution_convert_fusion.5
  107.6 1.6 %collective-permute-start.25 = (bf16[1024,512]{1,0:T(8,128)(2,1)S(1)}, bf16[1024,512]{1,0:T(8,128)(2,1)S(1)}, u32[]{:S(2)}, u32[]{:S(2)}) collective-permute-start(bf16[1024,512]{1,0:T(8,128)(2,1)S(1)} %get-tuple-element.9), channel_id=1, source_target_pairs={{0,16},{16,0},{1,17},{17,1},{2,18},{18,2},{3,19},{19,3},{4,20},{20... | collective-permute-start | bytes 3145736 | tf_op jit(solution)/shard_map/ppermute | solution.py:32
  109.2 8.1 %collective-permute-done.17 = bf16[256,512]{1,0:T(8,128)(2,1)S(1)} collective-permute-done((bf16[256,512]{1,0:T(8,128)(2,1)S(1)}, bf16[256,512]{1,0:T(8,128)(2,1)S(1)}, u32[]{:S(2)}, u32[]{:S(2)}) %collective-permute-start.17) | collective-permute-done | bytes 262176 | tf_op jit(solution)/shard_map/ppermute | solution.py:76
  117.3 1.3 fusion.16
  118.6 1.6 %collective-permute-start.20 = (bf16[512,1024]{1,0:T(8,128)(2,1)S(1)}, bf16[512,1024]{1,0:T(8,128)(2,1)S(1)}, u32[]{:S(2)}, u32[]{:S(2)}) collective-permute-start(bf16[512,1024]{1,0:T(8,128)(2,1)S(1)} %get-tuple-element.7), channel_id=1, source_target_pairs={{0,16},{16,0},{1,17},{17,1},{2,18},{18,2},{3,19},{19,3},{4,20},{20... | collective-permute-start | bytes 3145736 | tf_op jit(solution)/shard_map/ppermute | solution.py:32
  120.1 0.5 convolution_convert_fusion.6
  120.6 0.7 collective-permute-start.10
  121.6 8.5 %collective-permute-done.12 = bf16[256,512]{1,0:T(8,128)(2,1)S(1)} collective-permute-done((bf16[256,512]{1,0:T(8,128)(2,1)S(1)}, bf16[256,512]{1,0:T(8,128)(2,1)S(1)}, u32[]{:S(2)}, u32[]{:S(2)}) %collective-permute-start.12) | collective-permute-done | bytes 262176 | tf_op jit(solution)/shard_map/ppermute | solution.py:107
  130.1 0.5 fusion.20
  130.6 0.7 collective-permute-start.15
  131.3 2.4 %collective-permute-done.25 = bf16[1024,512]{1,0:T(8,128)(2,1)S(1)} collective-permute-done((bf16[1024,512]{1,0:T(8,128)(2,1)S(1)}, bf16[1024,512]{1,0:T(8,128)(2,1)S(1)}, u32[]{:S(2)}, u32[]{:S(2)}) %collective-permute-start.25) | collective-permute-done | bytes 1048608 | tf_op jit(solution)/shard_map/ppermute | solution.py:32
  133.7 1.7 %convert_add_fusion = f32[1024,512]{1,0:T(8,128)} fusion(bf16[1024,512]{1,0:T(8,128)(2,1)S(1)} %collective-permute-done.25, f32[1024,512]{1,0:T(8,128)S(1)} %get-tuple-element.10), kind=kLoop, calls=%fused_computation.16 | loop fusion | flops 2097152 | bytes 5242880 | tf_op jit(solution)/shard_map/add | solution.py:33
  135.4 14.2 %collective-permute-done.20 = bf16[512,1024]{1,0:T(8,128)(2,1)S(1)} collective-permute-done((bf16[512,1024]{1,0:T(8,128)(2,1)S(1)}, bf16[512,1024]{1,0:T(8,128)(2,1)S(1)}, u32[]{:S(2)}, u32[]{:S(2)}) %collective-permute-start.20) | collective-permute-done | bytes 1048608 | tf_op jit(solution)/shard_map/ppermute | solution.py:32
  149.5 1.7 %convert_add_fusion.1 = f32[512,1024]{1,0:T(8,128)} fusion(bf16[512,1024]{1,0:T(8,128)(2,1)S(1)} %collective-permute-done.20, f32[512,1024]{1,0:T(8,128)S(1)} %get-tuple-element.8), kind=kLoop, calls=%fused_computation.18 | loop fusion | flops 2097152 | bytes 5242880 | tf_op jit(solution)/shard_map/add | solution.py:33
  151.2 0.7 copy.11
  (32 shorter events, 1.2 us)
Async XLA Ops:
  2.4 2.4 %collective-permute-start = (bf16[256,512]{1,0:T(8,128)(2,1)S(1)}, bf16[256,512]{1,0:T(8,128)(2,1)S(1)}, u32[]{:S(2)}, u32[]{:S(2)}) collective-permute-start(bf16[256,512]{1,0:T(8,128)(2,1)S(1)} %multiply_convert_fusion.2), channel_id=1, source_target_pairs={{0,0},{4,1},{8,2},{12,3},{5,4},{9,5},{13,6},{1,7},{10,8},{14,9},{2... | collective-permute-start | bytes 786440 | tf_op jit(solution)/shard_map/ppermute | solution.py:72
  4.8 19.4 %collective-permute-start.6 = (bf16[256,512]{1,0:T(8,128)(2,1)S(1)}, bf16[256,512]{1,0:T(8,128)(2,1)S(1)}, u32[]{:S(2)}, u32[]{:S(2)}) collective-permute-start(bf16[256,512]{1,0:T(8,128)(2,1)S(1)} %collective-permute-done), channel_id=1, source_target_pairs={{0,3},{1,0},{2,1},{3,2},{4,7},{5,4},{6,5},{7,6},{8,11},{9,8},{10,9... | collective-permute-start | bytes 786440 | tf_op jit(solution)/shard_map/ppermute | solution.py:76
  20.8 30.6 %collective-permute-start.1 = (bf16[256,1024]{1,0:T(8,128)(2,1)S(1)}, bf16[256,1024]{1,0:T(8,128)(2,1)S(1)}, u32[]{:S(2)}, u32[]{:S(2)}) collective-permute-start(bf16[256,1024]{1,0:T(8,128)(2,1)S(1)} %convolution_convert_fusion.3), channel_id=1, source_target_pairs={{0,0},{1,5},{2,10},{3,15},{4,4},{5,9},{6,14},{7,3},{8,8},{9,13},{1... | collective-permute-start | bytes 1572872 | tf_op jit(solution)/shard_map/ppermute | solution.py:91
  21.5 20.8 %collective-permute-start.4 = (bf16[256,512]{1,0:T(8,128)(2,1)S(1)}, bf16[256,512]{1,0:T(8,128)(2,1)S(1)}, u32[]{:S(2)}, u32[]{:S(2)}) collective-permute-start(bf16[256,512]{1,0:T(8,128)(2,1)S(1)} %collective-permute-done), channel_id=1, source_target_pairs={{0,2},{1,3},{2,0},{3,1},{4,6},{5,7},{6,4},{7,5},{8,10},{9,11},{10,... | collective-permute-start | bytes 786440 | tf_op jit(solution)/shard_map/ppermute | solution.py:76
  23.8 21.9 %collective-permute-start.2 = (bf16[256,512]{1,0:T(8,128)(2,1)S(1)}, bf16[256,512]{1,0:T(8,128)(2,1)S(1)}, u32[]{:S(2)}, u32[]{:S(2)}) collective-permute-start(bf16[256,512]{1,0:T(8,128)(2,1)S(1)} %collective-permute-done), channel_id=1, source_target_pairs={{0,1},{1,2},{2,3},{3,0},{4,5},{5,6},{6,7},{7,4},{8,9},{9,10},{10,1... | collective-permute-start | bytes 786440 | tf_op jit(solution)/shard_map/ppermute | solution.py:76
  24.7 24.5 %copy-start.1 = (bf16[256,1024]{1,0:T(8,128)(2,1)S(1)}, bf16[256,1024]{1,0:T(8,128)(2,1)}, u32[]{:S(2)}) copy-start(bf16[256,1024]{1,0:T(8,128)(2,1)} %param.9) | copy-start | bytes 1572868
  24.7 44.5 %copy-start.3 = (bf16[256,512]{1,0:T(8,128)(2,1)S(1)}, bf16[256,512]{1,0:T(8,128)(2,1)}, u32[]{:S(2)}) copy-start(bf16[256,512]{1,0:T(8,128)(2,1)} %param.7) | copy-start | bytes 786436
  24.7 29.7 %collective-permute-start.7 = (bf16[256,1024]{1,0:T(8,128)(2,1)S(1)}, bf16[256,1024]{1,0:T(8,128)(2,1)S(1)}, u32[]{:S(2)}, u32[]{:S(2)}) collective-permute-start(bf16[256,1024]{1,0:T(8,128)(2,1)S(1)} %convolution_convert_fusion), channel_id=1, source_target_pairs={{0,4},{1,9},{2,14},{3,3},{4,8},{5,13},{6,2},{7,7},{8,12},{9,1},{10... | collective-permute-start | bytes 1572872 | tf_op jit(solution)/shard_map/ppermute | solution.py:91
  42.8 16.7 %collective-permute-start.5 = (bf16[256,1024]{1,0:T(8,128)(2,1)S(1)}, bf16[256,1024]{1,0:T(8,128)(2,1)S(1)}, u32[]{:S(2)}, u32[]{:S(2)}) collective-permute-start(bf16[256,1024]{1,0:T(8,128)(2,1)S(1)} %convolution_convert_fusion.1), channel_id=1, source_target_pairs={{0,8},{1,13},{2,2},{3,7},{4,12},{5,1},{6,6},{7,11},{8,0},{9,5},{10... | collective-permute-start | bytes 1572872 | tf_op jit(solution)/shard_map/ppermute | solution.py:91
  46.2 24.1 %copy-start.2 = (f32[1024]{0:T(1024)S(1)}, f32[1024]{0:T(1024)}, u32[]{:S(2)}) copy-start(f32[1024]{0:T(1024)} %param.11) | copy-start | bytes 12292
  46.2 23.0 %collective-permute-start.3 = (bf16[256,1024]{1,0:T(8,128)(2,1)S(1)}, bf16[256,1024]{1,0:T(8,128)(2,1)S(1)}, u32[]{:S(2)}, u32[]{:S(2)}) collective-permute-start(bf16[256,1024]{1,0:T(8,128)(2,1)S(1)} %convolution_convert_fusion.2), channel_id=1, source_target_pairs={{0,12},{1,1},{2,6},{3,11},{4,0},{5,5},{6,10},{7,15},{8,4},{9,9},{1... | collective-permute-start | bytes 1572872 | tf_op jit(solution)/shard_map/ppermute | solution.py:91
  49.4 33.0 %copy-start = (f32[512,1024]{1,0:T(8,128)S(1)}, f32[512,1024]{1,0:T(8,128)}, u32[]{:S(2)}) copy-start(f32[512,1024]{1,0:T(8,128)} %param.10) | copy-start | bytes 6291460
  49.4 33.1 %collective-permute-start.24 = (bf16[256,1024]{1,0:T(8,128)(2,1)S(1)}, bf16[256,1024]{1,0:T(8,128)(2,1)S(1)}, u32[]{:S(2)}, u32[]{:S(2)}) collective-permute-start(bf16[256,1024]{1,0:T(8,128)(2,1)S(1)} %multiply_convert_fusion), channel_id=1, source_target_pairs={{4,0},{9,1},{14,2},{3,3},{8,4},{13,5},{2,6},{7,7},{12,8},{1,9},{6,... | collective-permute-start | bytes 1572872 | tf_op jit(solution)/shard_map/ppermute | solution.py:96
  51.5 35.9 %collective-permute-start.23 = (bf16[256,1024]{1,0:T(8,128)(2,1)S(1)}, bf16[256,1024]{1,0:T(8,128)(2,1)S(1)}, u32[]{:S(2)}, u32[]{:S(2)}) collective-permute-start(bf16[256,1024]{1,0:T(8,128)(2,1)S(1)} %multiply_convert_fusion), channel_id=1, source_target_pairs={{8,0},{13,1},{2,2},{7,3},{12,4},{1,5},{6,6},{11,7},{0,8},{5,9},{10... | collective-permute-start | bytes 1572872 | tf_op jit(solution)/shard_map/ppermute | solution.py:96
  54.4 32.9 %collective-permute-start.22 = (bf16[256,1024]{1,0:T(8,128)(2,1)S(1)}, bf16[256,1024]{1,0:T(8,128)(2,1)S(1)}, u32[]{:S(2)}, u32[]{:S(2)}) collective-permute-start(bf16[256,1024]{1,0:T(8,128)(2,1)S(1)} %multiply_convert_fusion), channel_id=1, source_target_pairs={{12,0},{1,1},{6,2},{11,3},{0,4},{5,5},{10,6},{15,7},{4,8},{9,9},{1... | collective-permute-start | bytes 1572872 | tf_op jit(solution)/shard_map/ppermute | solution.py:96
  59.5 30.2 %collective-permute-start.21 = (bf16[256,1024]{1,0:T(8,128)(2,1)S(1)}, bf16[256,1024]{1,0:T(8,128)(2,1)S(1)}, u32[]{:S(2)}, u32[]{:S(2)}) collective-permute-start(bf16[256,1024]{1,0:T(8,128)(2,1)S(1)} %multiply_convert_fusion), channel_id=1, source_target_pairs={{0,0},{5,1},{10,2},{15,3},{4,4},{9,5},{14,6},{3,7},{8,8},{13,9},{2... | collective-permute-start | bytes 1572872 | tf_op jit(solution)/shard_map/ppermute | solution.py:96
  69.2 1.2 collective-permute-start.16
  70.5 23.3 %collective-permute-start.13 = (bf16[256,1024]{1,0:T(8,128)(2,1)S(1)}, bf16[256,1024]{1,0:T(8,128)(2,1)S(1)}, u32[]{:S(2)}, u32[]{:S(2)}) collective-permute-start(bf16[256,1024]{1,0:T(8,128)(2,1)S(1)} %multiply_convert_fusion.1), channel_id=1, source_target_pairs={{4,0},{9,1},{14,2},{3,3},{8,4},{13,5},{2,6},{7,7},{12,8},{1,9},{6,... | collective-permute-start | bytes 1572872 | tf_op jit(solution)/shard_map/ppermute | solution.py:102
  82.5 25.1 %collective-permute-start.19 = (bf16[256,512]{1,0:T(8,128)(2,1)S(1)}, bf16[256,512]{1,0:T(8,128)(2,1)S(1)}, u32[]{:S(2)}, u32[]{:S(2)}) collective-permute-start(bf16[256,512]{1,0:T(8,128)(2,1)S(1)} %collective-permute-done.16), channel_id=1, source_target_pairs={{0,3},{1,0},{2,1},{3,2},{4,7},{5,4},{6,5},{7,6},{8,11},{9,8},{10,9... | collective-permute-start | bytes 786440 | tf_op jit(solution)/shard_map/ppermute | solution.py:76
  87.4 21.8 %collective-permute-start.18 = (bf16[256,512]{1,0:T(8,128)(2,1)S(1)}, bf16[256,512]{1,0:T(8,128)(2,1)S(1)}, u32[]{:S(2)}, u32[]{:S(2)}) collective-permute-start(bf16[256,512]{1,0:T(8,128)(2,1)S(1)} %collective-permute-done.16), channel_id=1, source_target_pairs={{0,2},{1,3},{2,0},{3,1},{4,6},{5,7},{6,4},{7,5},{8,10},{9,11},{10,... | collective-permute-start | bytes 786440 | tf_op jit(solution)/shard_map/ppermute | solution.py:76
  87.4 19.7 %collective-permute-start.11 = (bf16[256,1024]{1,0:T(8,128)(2,1)S(1)}, bf16[256,1024]{1,0:T(8,128)(2,1)S(1)}, u32[]{:S(2)}, u32[]{:S(2)}) collective-permute-start(bf16[256,1024]{1,0:T(8,128)(2,1)S(1)} %multiply_convert_fusion.1), channel_id=1, source_target_pairs={{8,0},{13,1},{2,2},{7,3},{12,4},{1,5},{6,6},{11,7},{0,8},{5,9},{10... | collective-permute-start | bytes 1572872 | tf_op jit(solution)/shard_map/ppermute | solution.py:102
  90.9 26.3 %collective-permute-start.8 = (bf16[256,1024]{1,0:T(8,128)(2,1)S(1)}, bf16[256,1024]{1,0:T(8,128)(2,1)S(1)}, u32[]{:S(2)}, u32[]{:S(2)}) collective-permute-start(bf16[256,1024]{1,0:T(8,128)(2,1)S(1)} %multiply_convert_fusion.1), channel_id=1, source_target_pairs={{0,0},{5,1},{10,2},{15,3},{4,4},{9,5},{14,6},{3,7},{8,8},{13,9},{2... | collective-permute-start | bytes 1572872 | tf_op jit(solution)/shard_map/ppermute | solution.py:102
  93.8 23.5 %collective-permute-start.9 = (bf16[256,1024]{1,0:T(8,128)(2,1)S(1)}, bf16[256,1024]{1,0:T(8,128)(2,1)S(1)}, u32[]{:S(2)}, u32[]{:S(2)}) collective-permute-start(bf16[256,1024]{1,0:T(8,128)(2,1)S(1)} %multiply_convert_fusion.1), channel_id=1, source_target_pairs={{12,0},{1,1},{6,2},{11,3},{0,4},{5,5},{10,6},{15,7},{4,8},{9,9},{1... | collective-permute-start | bytes 1572872 | tf_op jit(solution)/shard_map/ppermute | solution.py:102
  107.1 10.2 %collective-permute-start.17 = (bf16[256,512]{1,0:T(8,128)(2,1)S(1)}, bf16[256,512]{1,0:T(8,128)(2,1)S(1)}, u32[]{:S(2)}, u32[]{:S(2)}) collective-permute-start(bf16[256,512]{1,0:T(8,128)(2,1)S(1)} %collective-permute-done.16), channel_id=1, source_target_pairs={{0,1},{1,2},{2,3},{3,0},{4,5},{5,6},{6,7},{7,4},{8,9},{9,10},{10,1... | collective-permute-start | bytes 786440 | tf_op jit(solution)/shard_map/ppermute | solution.py:76
  107.6 26.1 %collective-permute-start.25 = (bf16[1024,512]{1,0:T(8,128)(2,1)S(1)}, bf16[1024,512]{1,0:T(8,128)(2,1)S(1)}, u32[]{:S(2)}, u32[]{:S(2)}) collective-permute-start(bf16[1024,512]{1,0:T(8,128)(2,1)S(1)} %get-tuple-element.9), channel_id=1, source_target_pairs={{0,16},{16,0},{1,17},{17,1},{2,18},{18,2},{3,19},{19,3},{4,20},{20... | collective-permute-start | bytes 3145736 | tf_op jit(solution)/shard_map/ppermute | solution.py:32
  109.1 12.4 %collective-permute-start.14 = (bf16[256,512]{1,0:T(8,128)(2,1)S(1)}, bf16[256,512]{1,0:T(8,128)(2,1)S(1)}, u32[]{:S(2)}, u32[]{:S(2)}) collective-permute-start(bf16[256,512]{1,0:T(8,128)(2,1)S(1)} %convolution_convert_fusion.4), channel_id=1, source_target_pairs={{0,1},{1,2},{2,3},{3,0},{4,5},{5,6},{6,7},{7,4},{8,9},{9,10},{10,1... | collective-permute-start | bytes 786440 | tf_op jit(solution)/shard_map/ppermute | solution.py:107
  117.3 12.8 %collective-permute-start.12 = (bf16[256,512]{1,0:T(8,128)(2,1)S(1)}, bf16[256,512]{1,0:T(8,128)(2,1)S(1)}, u32[]{:S(2)}, u32[]{:S(2)}) collective-permute-start(bf16[256,512]{1,0:T(8,128)(2,1)S(1)} %convolution_convert_fusion.5), channel_id=1, source_target_pairs={{0,2},{1,3},{2,0},{3,1},{4,6},{5,7},{6,4},{7,5},{8,10},{9,11},{10,... | collective-permute-start | bytes 786440 | tf_op jit(solution)/shard_map/ppermute | solution.py:107
  118.6 31.0 %collective-permute-start.20 = (bf16[512,1024]{1,0:T(8,128)(2,1)S(1)}, bf16[512,1024]{1,0:T(8,128)(2,1)S(1)}, u32[]{:S(2)}, u32[]{:S(2)}) collective-permute-start(bf16[512,1024]{1,0:T(8,128)(2,1)S(1)} %get-tuple-element.7), channel_id=1, source_target_pairs={{0,16},{16,0},{1,17},{17,1},{2,18},{18,2},{3,19},{19,3},{4,20},{20... | collective-permute-start | bytes 3145736 | tf_op jit(solution)/shard_map/ppermute | solution.py:32
  120.6 9.5 %collective-permute-start.10 = (bf16[256,512]{1,0:T(8,128)(2,1)S(1)}, bf16[256,512]{1,0:T(8,128)(2,1)S(1)}, u32[]{:S(2)}, u32[]{:S(2)}) collective-permute-start(bf16[256,512]{1,0:T(8,128)(2,1)S(1)} %convolution_convert_fusion.6), channel_id=1, source_target_pairs={{0,3},{1,0},{2,1},{3,2},{4,7},{5,4},{6,5},{7,6},{8,11},{9,8},{10,9... | collective-permute-start | bytes 786440 | tf_op jit(solution)/shard_map/ppermute | solution.py:107
  130.6 4.7 %collective-permute-start.15 = (bf16[256,512]{1,0:T(8,128)(2,1)S(1)}, bf16[256,512]{1,0:T(8,128)(2,1)S(1)}, u32[]{:S(2)}, u32[]{:S(2)}) collective-permute-start(bf16[256,512]{1,0:T(8,128)(2,1)S(1)} %fusion.20), channel_id=1, source_target_pairs={{0,0},{1,4},{2,8},{3,12},{4,5},{5,9},{6,13},{7,1},{8,10},{9,14},{1... | collective-permute-start | bytes 786440 | tf_op jit(solution)/shard_map/ppermute | solution.py:111
where the time goes:
time: 153 us; the launch traced here: 152 us
  waiting for transfers between devices  74.1 us (48%)
  starting transfers between devices  62 us (41%)
  other arithmetic  6.93 us (5%)
  matrix products  6.38 us (4%)
    ppermute x6, waiting for transfers between devices, to_features(): lax.ppermute(base[a], 'tp', [(i, (i + s) % nt) for i in range(nt)])  21.9 us
    ppermute x4, starting transfers between devices, body(): lax.ppermute(d_pre, BOTH, from_owner(s, a))  18.9 us
    ppermute x6, starting transfers between devices, to_features(): lax.ppermute(base[a], 'tp', [(i, (i + s) % nt) for i in range(nt)])  18.9 us
    ppermute x2, waiting for transfers between devices, rep_sum(): other = lax.ppermute(own.astype(jnp.bfloat16), 'rep', [(0, 1), (1, 0)])  16.5 us
    ppermute x4, waiting for transfers between devices, body(): lax.ppermute(partial_value, BOTH, to_owner(s, a)).astype(jnp.float32)  12.2 us
    ppermute x4, waiting for transfers between devices, body(): lax.ppermute(d_pre, BOTH, from_owner(s, a))  10.9 us
    ppermute x4, starting transfers between devices, body(): lax.ppermute(partial_value, BOTH, to_owner(s, a)).astype(jnp.float32)  10.9 us
    ppermute x3, waiting for transfers between devices, body(): lax.ppermute(value.astype(jnp.bfloat16), 'tp', [(i, (i - s) % nt) for i i...  8.79 us
  transfers between devices with their start and end apart: 26, of which 12 were waited for; matrix products, arithmetic and copies ran while one was open for 7% of the time, Pallas kernels for 0%

commit v1 on v0

--- a/solution.py
+++ b/solution.py
@@ -25,11 +25,15 @@
     return lax.reduce_precision(x, exponent_bits=8, mantissa_bits=7)
 
 
+def move(x, axis, pairs):
+    return lax.ppermute(x, axis, pairs)
+
+
 def rep_sum(x):
     if lax.axis_size("rep") != 2:
         return lax.psum(x, "rep")
     own = round_bf16(x)
-    other = lax.ppermute(own.astype(jnp.bfloat16), "rep", [(0, 1), (1, 0)])
+    other = move(own.astype(jnp.bfloat16), "rep", [(0, 1), (1, 0)])
     return own + other.astype(jnp.float32)
 
 
@@ -43,7 +47,7 @@
     slots = [(s, a) for s in range(nt) for a in range(per)]
 
     def token_block(fi, ti, s, a):
-        return (fi + (ti - s) * per + a) % nf
+        return fi ^ ((ti ^ s) * per + a)
 
     def grid(target):
         return [
@@ -53,8 +57,19 @@
     def to_owner(s, a):
         return grid(lambda fi, ti: token_block(fi, ti, s, a) * nt + ti)
 
-    def from_owner(s, a):
-        return [(dst, src) for src, dst in to_owner(s, a)]
+    def all_tokens(x):
+        blocks = [x]
+        for i in range(1, nf):
+            source, step = (blocks[i - 1], 1) if i % 2 else (x, i)
+            blocks.append(move(source, "fs", [(j, j ^ step) for j in range(nf)]))
+        return jnp.concatenate(blocks)
+
+    def by_place(blocks):
+        stack = jnp.concatenate(blocks)
+        rows = per * tok
+        return jnp.concatenate(
+            [lax.dynamic_slice_in_dim(stack, (t ^ s) * rows, rows, 0) for s in range(nt)]
+        )
 
     def home(a):
         return grid(lambda fi, ti: token_block(fi, ti, 0, a) * nt + fi // per)
@@ -63,17 +78,17 @@
         return [(dst, src) for src, dst in home(a)]
 
     def part_at(a):
-        return ((f - a) % per) * width
+        return ((f % per) ^ a) * width
 
     def to_features(x):
         base = []
         for a in range(per):
             piece = x if per == 1 else lax.dynamic_slice_in_dim(x, part_at(a), width, 1)
-            base.append(lax.ppermute(piece, BOTH, away(a)))
+            base.append(move(piece, BOTH, away(a)))
         return [
             base[a]
             if s == 0
-            else lax.ppermute(base[a], "tp", [(i, (i + s) % nt) for i in range(nt)])
+            else move(base[a], "tp", [(i, i ^ s) for i in range(nt)])
             for s, a in slots
         ]
 
@@ -88,27 +103,28 @@
     d_act = 0.0
     for (s, a), block in zip(slots, scaled_blocks):
         partial_value = contract_last(block, down_bf).astype(jnp.bfloat16)
-        d_act += lax.ppermute(partial_value, BOTH, to_owner(s, a)).astype(jnp.float32)
+        d_act += move(partial_value, BOTH, to_owner(s, a)).astype(jnp.float32)
     late_pre, d_act = lax.optimization_barrier((pre_act, d_act))
     positive = jnp.maximum(late_pre.astype(jnp.float32), 0.0)
     d_pre = (2.0 * positive * d_act * up_scale[None, :]).astype(jnp.bfloat16)
 
-    act_blocks = [lax.ppermute(act, BOTH, from_owner(s, a)) for s, a in slots]
+    act_all = all_tokens(act)
     acts_blocks = to_features(acts)
-    grad_down = rep_sum(
-        contract_first(jnp.concatenate(act_blocks), jnp.concatenate(scaled_blocks)) * norm_factor
-    )
+    scaled_all = by_place(scaled_blocks)
+    down_part = contract_first(act_all, scaled_all) * norm_factor
+    grad_down = rep_sum(down_part)
 
-    dpre_blocks = [lax.ppermute(d_pre, BOTH, from_owner(s, a)) for s, a in slots]
+    dpre_all = all_tokens(d_pre)
     sums = [0.0] * per
-    for (s, a), block in zip(slots, dpre_blocks):
+    for s, a in slots:
+        block = lax.dynamic_slice_in_dim(dpre_all, ((t ^ s) * per + a) * tok, tok, 0)
         value = contract_last(block, up_bf)
         if s:
-            value = lax.ppermute(
-                value.astype(jnp.bfloat16), "tp", [(i, (i - s) % nt) for i in range(nt)]
+            value = move(
+                value.astype(jnp.bfloat16), "tp", [(i, i ^ s) for i in range(nt)]
             ).astype(jnp.float32)
         sums[a] += value
-    pieces = [lax.ppermute(sums[a].astype(jnp.bfloat16), BOTH, home(a)) for a in range(per)]
+    pieces = [move(sums[a].astype(jnp.bfloat16), BOTH, home(a)) for a in range(per)]
     if per == 1:
         grad_input = pieces[0]
     else:
@@ -116,9 +132,7 @@
         for a in range(per):
             grad_input = lax.dynamic_update_slice_in_dim(grad_input, pieces[a], part_at(a), 1)
 
-    grad_up = rep_sum(
-        contract_first(jnp.concatenate(acts_blocks), jnp.concatenate(dpre_blocks)) * norm_factor
-    )
+    grad_up = rep_sum(contract_first(by_place(acts_blocks), dpre_all) * norm_factor)
     return (grad_input, grad_up, grad_down)
 
 

time: 153 us -> 151 us (0.987)
  the two profiles are of different devices: /device:TPU:0 before, /device:TPU:20 now
where the time goes in v1:
time: 151 us; the launch traced here: 150 us
  waiting for transfers between devices  79.5 us (53%)
  starting transfers between devices  44.5 us (29%)
  matrix products  9.63 us (6%)
  other arithmetic  9.49 us (6%)
  local copies, waits for them, and re-layouts  5.66 us (4%)
    ppermute x24, waiting for transfers between devices, move(): return lax.ppermute(x, axis, pairs)  79.5 us
    ppermute x24, starting transfers between devices, move(): return lax.ppermute(x, axis, pairs)  44.5 us
    dot_general x8, matrix products, contract_last(): lax.dot_general(left, right, (((1,), (1,)), ((), ())), preferred_element_...  7.06 us
    unnamed x23, local copies, waits for them, and re-layouts  4.7 us
    add x2, other arithmetic, rep_sum(): return own + other.astype(jnp.float32)  3.47 us
  transfers between devices with their start and end apart: 24, of which 9 were waited for; matrix products, arithmetic and copies ran while one was open for 14% of the time, Pallas kernels for 0%

profile of v1, /device:TPU:20, one launch (start us, length us, event | category | flops | bytes accessed | tf_op | source)
XLA Modules:
  0.0 149.8 jit_solution(1384856414918903960)
XLA Ops:
  0.6 0.8 dynamic_slice.39
  1.4 1.0 multiply_convert_fusion.2
  2.4 2.2 %collective-permute-start = (bf16[256,512]{1,0:T(8,128)(2,1)S(1)}, bf16[256,512]{1,0:T(8,128)(2,1)S(1)}, u32[]{:S(2)}, u32[]{:S(2)}) collective-permute-start(bf16[256,512]{1,0:T(8,128)(2,1)S(1)} %multiply_convert_fusion.2), channel_id=1, source_target_pairs={{0,0},{4,1},{8,2},{12,3},{5,4},{1,5},{13,6},{9,7},{10,8},{14,9},{2... | collective-permute-start | bytes 786440 | tf_op jit(solution)/shard_map/ppermute | solution.py:29
  4.6 4.4 %collective-permute-start.15 = (bf16[256,512]{1,0:T(8,128)(2,1)}, bf16[256,512]{1,0:T(8,128)(2,1)}, u32[]{:S(2)}, u32[]{:S(2)}) collective-permute-start(bf16[256,512]{1,0:T(8,128)(2,1)} %param.7), channel_id=1, source_target_pairs={{0,0},{4,1},{8,2},{12,3},{5,4},{1,5},{13,6},{9,7},{10,8},{14,9},{2... | collective-permute-start | bytes 786440 | tf_op jit(solution)/shard_map/ppermute | solution.py:29
  9.1 1.7 %convert_element_type.83 = bf16[1024,512]{1,0:T(8,128)(2,1)S(1)} convert(f32[1024,512]{1,0:T(8,128)} %param.12) | non-fusion elementwise | flops 524288 | bytes 3145728 | tf_op jit(solution)/shard_map/convert_element_type | solution.py:100
  10.8 14.5 %collective-permute-done = bf16[256,512]{1,0:T(8,128)(2,1)S(1)} collective-permute-done((bf16[256,512]{1,0:T(8,128)(2,1)S(1)}, bf16[256,512]{1,0:T(8,128)(2,1)S(1)}, u32[]{:S(2)}, u32[]{:S(2)}) %collective-permute-start) | collective-permute-done | bytes 262176 | tf_op jit(solution)/shard_map/ppermute | solution.py:29
  25.3 2.2 %collective-permute-start.6 = (bf16[256,512]{1,0:T(8,128)(2,1)S(1)}, bf16[256,512]{1,0:T(8,128)(2,1)S(1)}, u32[]{:S(2)}, u32[]{:S(2)}) collective-permute-start(bf16[256,512]{1,0:T(8,128)(2,1)S(1)} %collective-permute-done), channel_id=1, source_target_pairs={{0,3},{1,2},{2,1},{3,0},{4,7},{5,6},{6,5},{7,4},{8,11},{9,10},{10,... | collective-permute-start | bytes 786440 | tf_op jit(solution)/shard_map/ppermute | solution.py:29
  27.5 1.3 convolution_convert_fusion.3
  28.7 1.9 %collective-permute-start.1 = (bf16[256,1024]{1,0:T(8,128)(2,1)}, bf16[256,1024]{1,0:T(8,128)(2,1)}, u32[]{:S(2)}, u32[]{:S(2)}) collective-permute-start(bf16[256,1024]{1,0:T(8,128)(2,1)} %convolution_convert_fusion.3), channel_id=1, source_target_pairs={{0,0},{1,5},{2,10},{3,15},{4,4},{5,1},{6,14},{7,11},{8,8},{9,13},{... | collective-permute-start | bytes 1572872 | tf_op jit(solution)/shard_map/ppermute | solution.py:29
  30.6 4.7 %collective-permute-start.4 = (bf16[256,512]{1,0:T(8,128)(2,1)S(1)}, bf16[256,512]{1,0:T(8,128)(2,1)S(1)}, u32[]{:S(2)}, u32[]{:S(2)}) collective-permute-start(bf16[256,512]{1,0:T(8,128)(2,1)S(1)} %collective-permute-done), channel_id=1, source_target_pairs={{0,2},{1,3},{2,0},{3,1},{4,6},{5,7},{6,4},{7,5},{8,10},{9,11},{10,... | collective-permute-start | bytes 786440 | tf_op jit(solution)/shard_map/ppermute | solution.py:29
  35.3 12.3 %collective-permute-done.6 = bf16[256,512]{1,0:T(8,128)(2,1)S(1)} collective-permute-done((bf16[256,512]{1,0:T(8,128)(2,1)S(1)}, bf16[256,512]{1,0:T(8,128)(2,1)S(1)}, u32[]{:S(2)}, u32[]{:S(2)}) %collective-permute-start.6) | collective-permute-done | bytes 262176 | tf_op jit(solution)/shard_map/ppermute | solution.py:29
  47.6 1.3 convolution_convert_fusion
  48.9 2.2 %collective-permute-start.7 = (bf16[256,1024]{1,0:T(8,128)(2,1)}, bf16[256,1024]{1,0:T(8,128)(2,1)}, u32[]{:S(2)}, u32[]{:S(2)}) collective-permute-start(bf16[256,1024]{1,0:T(8,128)(2,1)} %convolution_convert_fusion), channel_id=1, source_target_pairs={{0,12},{1,9},{2,6},{3,3},{4,8},{5,13},{6,2},{7,7},{8,4},{9,1},{10,... | collective-permute-start | bytes 1572872 | tf_op jit(solution)/shard_map/ppermute | solution.py:29
  51.1 1.3 convolution_convert_fusion.1
  52.3 5.3 %collective-permute-start.5 = (bf16[256,1024]{1,0:T(8,128)(2,1)}, bf16[256,1024]{1,0:T(8,128)(2,1)}, u32[]{:S(2)}, u32[]{:S(2)}) collective-permute-start(bf16[256,1024]{1,0:T(8,128)(2,1)} %convolution_convert_fusion.1), channel_id=1, source_target_pairs={{0,8},{1,13},{2,2},{3,7},{4,12},{5,9},{6,6},{7,3},{8,0},{9,5},{10,... | collective-permute-start | bytes 1572872 | tf_op jit(solution)/shard_map/ppermute | solution.py:29
  57.7 1.3 convolution_convert_fusion.2
  59.0 1.9 %collective-permute-start.3 = (bf16[256,1024]{1,0:T(8,128)(2,1)}, bf16[256,1024]{1,0:T(8,128)(2,1)}, u32[]{:S(2)}, u32[]{:S(2)}) collective-permute-start(bf16[256,1024]{1,0:T(8,128)(2,1)} %convolution_convert_fusion.2), channel_id=1, source_target_pairs={{0,4},{1,1},{2,14},{3,11},{4,0},{5,5},{6,10},{7,15},{8,12},{9,9},{... | collective-permute-start | bytes 1572872 | tf_op jit(solution)/shard_map/ppermute | solution.py:29
  60.9 0.9 multiply_convert_fusion
  62.0 1.0 constant_dynamic-update-slice_fusion.7
  63.0 2.2 %collective-permute-start.21 = (bf16[256,1024]{1,0:T(8,128)(2,1)}, bf16[256,1024]{1,0:T(8,128)(2,1)S(1)}, u32[]{:S(2)}, u32[]{:S(2)}) collective-permute-start(bf16[256,1024]{1,0:T(8,128)(2,1)} %multiply_convert_fusion), channel_id=1, source_target_pairs={{0,8},{4,12},{8,0},{12,4},{1,9},{5,13},{9,1},{13,5},{2,10},{6,14},... | collective-permute-start | bytes 1572872 | tf_op jit(solution)/shard_map/ppermute | solution.py:29
  65.2 1.0 constant_dynamic-update-slice_fusion.3
  66.2 1.0 constant_dynamic-update-slice_fusion.6
  67.2 1.0 constant_dynamic-update-slice_fusion.5
  68.3 1.2 collective-permute-start.17
  69.5 5.3 %collective-permute-start.18 = (bf16[256,512]{1,0:T(8,128)(2,1)}, bf16[256,512]{1,0:T(8,128)(2,1)S(1)}, u32[]{:S(2)}, u32[]{:S(2)}) collective-permute-start(bf16[256,512]{1,0:T(8,128)(2,1)} %collective-permute-done.15), channel_id=1, source_target_pairs={{0,3},{1,2},{2,1},{3,0},{4,7},{5,6},{6,5},{7,4},{8,11},{9,10},{10,... | collective-permute-start | bytes 786440 | tf_op jit(solution)/shard_map/ppermute | solution.py:29
  74.8 1.8 %convert_add_fusion.2 = f32[256,1024]{1,0:T(8,128)S(1)} fusion(bf16[256,1024]{1,0:T(8,128)(2,1)} %collective-permute-done.7, bf16[256,1024]{1,0:T(8,128)(2,1)} %collective-permute-done.5, bf16[256,1024]{1,0:T(8,128)(2,1)} %collective-permute-done.3, bf16[256,1024]{1,0:T(8,128)(2,1)} %collective-permute-done.1), kind=kLoop, calls=%fused_computation.43 | loop fusion | flops 1835008 | bytes 3145728 | tf_op jit(solution)/shard_map/add | solution.py:106
  76.8 2.1 %collective-permute-start.9 = (bf16[256,1024]{1,0:T(8,128)(2,1)S(1)}, bf16[256,1024]{1,0:T(8,128)(2,1)S(1)}, u32[]{:S(2)}, u32[]{:S(2)}) collective-permute-start(bf16[256,1024]{1,0:T(8,128)(2,1)S(1)} %multiply_convert_fusion.1), channel_id=1, source_target_pairs={{0,8},{4,12},{8,0},{12,4},{1,9},{5,13},{9,1},{13,5},{2,10},{6,14},... | collective-permute-start | bytes 1572872 | tf_op jit(solution)/shard_map/ppermute | solution.py:29
  79.0 0.9 collective-permute-start.20
  79.9 7.3 %collective-permute-done.21 = bf16[256,1024]{1,0:T(8,128)(2,1)S(1)} collective-permute-done((bf16[256,1024]{1,0:T(8,128)(2,1)}, bf16[256,1024]{1,0:T(8,128)(2,1)S(1)}, u32[]{:S(2)}, u32[]{:S(2)}) %collective-permute-start.21) | collective-permute-done | bytes 524320 | tf_op jit(solution)/shard_map/ppermute | solution.py:29
  87.3 7.2 %collective-permute-done.18 = bf16[256,512]{1,0:T(8,128)(2,1)S(1)} collective-permute-done((bf16[256,512]{1,0:T(8,128)(2,1)}, bf16[256,512]{1,0:T(8,128)(2,1)S(1)}, u32[]{:S(2)}, u32[]{:S(2)}) %collective-permute-start.18) | collective-permute-done | bytes 262176 | tf_op jit(solution)/shard_map/ppermute | solution.py:29
  94.7 3.1 %collective-permute-done.9 = bf16[256,1024]{1,0:T(8,128)(2,1)S(1)} collective-permute-done((bf16[256,1024]{1,0:T(8,128)(2,1)S(1)}, bf16[256,1024]{1,0:T(8,128)(2,1)S(1)}, u32[]{:S(2)}, u32[]{:S(2)}) %collective-permute-start.9) | collective-permute-done | bytes 524320 | tf_op jit(solution)/shard_map/ppermute | solution.py:29
  97.9 1.3 fusion.9
  99.2 1.6 %collective-permute-start.23 = (bf16[1024,512]{1,0:T(8,128)(2,1)S(1)}, bf16[1024,512]{1,0:T(8,128)(2,1)S(1)}, u32[]{:S(2)}, u32[]{:S(2)}) collective-permute-start(bf16[1024,512]{1,0:T(8,128)(2,1)S(1)} %get-tuple-element.17), channel_id=1, source_target_pairs={{0,16},{16,0},{1,17},{17,1},{2,18},{18,2},{3,19},{19,3},{4,20},{20... | collective-permute-start | bytes 3145736 | tf_op jit(solution)/shard_map/ppermute | solution.py:29
  100.7 1.3 fusion.8
  102.0 0.6 collective-permute-start.19
  102.8 0.5 convolution_convert_fusion.4
  103.3 0.5 convolution_convert_fusion.5
  104.5 0.9 collective-permute-start.12
  105.4 2.4 %collective-permute-start.11 = (bf16[256,512]{1,0:T(8,128)(2,1)S(1)}, bf16[256,512]{1,0:T(8,128)(2,1)S(1)}, u32[]{:S(2)}, u32[]{:S(2)}) collective-permute-start(bf16[256,512]{1,0:T(8,128)(2,1)S(1)} %convolution_convert_fusion.6), channel_id=1, source_target_pairs={{0,1},{1,0},{2,3},{3,2},{4,5},{5,4},{6,7},{7,6},{8,9},{9,8},{10,11... | collective-permute-start | bytes 786440 | tf_op jit(solution)/shard_map/ppermute | solution.py:29
  107.8 15.0 %collective-permute-done.13 = bf16[256,512]{1,0:T(8,128)(2,1)S(1)} collective-permute-done((bf16[256,512]{1,0:T(8,128)(2,1)S(1)}, bf16[256,512]{1,0:T(8,128)(2,1)S(1)}, u32[]{:S(2)}, u32[]{:S(2)}) %collective-permute-start.13) | collective-permute-done | bytes 262176 | tf_op jit(solution)/shard_map/ppermute | solution.py:29
  122.8 2.4 %collective-permute-done.12 = bf16[256,512]{1,0:T(8,128)(2,1)S(1)} collective-permute-done((bf16[256,512]{1,0:T(8,128)(2,1)S(1)}, bf16[256,512]{1,0:T(8,128)(2,1)S(1)}, u32[]{:S(2)}, u32[]{:S(2)}) %collective-permute-start.12) | collective-permute-done | bytes 262176 | tf_op jit(solution)/shard_map/ppermute | solution.py:29
  125.3 0.5 fusion.12
  125.8 2.2 %collective-permute-start.14 = (bf16[256,512]{1,0:T(8,128)(2,1)S(1)}, bf16[256,512]{1,0:T(8,128)(2,1)S(1)}, u32[]{:S(2)}, u32[]{:S(2)}) collective-permute-start(bf16[256,512]{1,0:T(8,128)(2,1)S(1)} %fusion.12), channel_id=1, source_target_pairs={{0,0},{1,4},{2,8},{3,12},{4,5},{5,1},{6,13},{7,9},{8,10},{9,14},{1... | collective-permute-start | bytes 786440 | tf_op jit(solution)/shard_map/ppermute | solution.py:29
  128.0 1.7 %convert_add_fusion = f32[1024,512]{1,0:T(8,128)} fusion(bf16[1024,512]{1,0:T(8,128)(2,1)S(1)} %collective-permute-done.23, f32[1024,512]{1,0:T(8,128)S(1)} %get-tuple-element.18), kind=kLoop, calls=%fused_computation.9 | loop fusion | flops 2097152 | bytes 5242880 | tf_op jit(solution)/shard_map/add | solution.py:37
  129.7 6.1 %collective-permute-done.14 = bf16[256,512]{1,0:T(8,128)(2,1)S(1)} collective-permute-done((bf16[256,512]{1,0:T(8,128)(2,1)S(1)}, bf16[256,512]{1,0:T(8,128)(2,1)S(1)}, u32[]{:S(2)}, u32[]{:S(2)}) %collective-permute-start.14) | collective-permute-done | bytes 262176 | tf_op jit(solution)/shard_map/ppermute | solution.py:29
  135.8 11.5 %collective-permute-done.19 = bf16[512,1024]{1,0:T(8,128)(2,1)S(1)} collective-permute-done((bf16[512,1024]{1,0:T(8,128)(2,1)S(1)}, bf16[512,1024]{1,0:T(8,128)(2,1)S(1)}, u32[]{:S(2)}, u32[]{:S(2)}) %collective-permute-start.19) | collective-permute-done | bytes 1048608 | tf_op jit(solution)/shard_map/ppermute | solution.py:29
  147.3 1.8 %convert_add_fusion.1 = f32[512,1024]{1,0:T(8,128)} fusion(bf16[512,1024]{1,0:T(8,128)(2,1)S(1)} %collective-permute-done.19, f32[512,1024]{1,0:T(8,128)S(1)} %get-tuple-element.16), kind=kLoop, calls=%fused_computation.11 | loop fusion | flops 2097152 | bytes 5242880 | tf_op jit(solution)/shard_map/add | solution.py:37
  149.1 0.7 copy.17
  (47 shorter events, 1.7 us)
Async XLA Ops:
  2.4 22.9 %collective-permute-start = (bf16[256,512]{1,0:T(8,128)(2,1)S(1)}, bf16[256,512]{1,0:T(8,128)(2,1)S(1)}, u32[]{:S(2)}, u32[]{:S(2)}) collective-permute-start(bf16[256,512]{1,0:T(8,128)(2,1)S(1)} %multiply_convert_fusion.2), channel_id=1, source_target_pairs={{0,0},{4,1},{8,2},{12,3},{5,4},{1,5},{13,6},{9,7},{10,8},{14,9},{2... | collective-permute-start | bytes 786440 | tf_op jit(solution)/shard_map/ppermute | solution.py:29
  4.6 58.3 %collective-permute-start.15 = (bf16[256,512]{1,0:T(8,128)(2,1)}, bf16[256,512]{1,0:T(8,128)(2,1)}, u32[]{:S(2)}, u32[]{:S(2)}) collective-permute-start(bf16[256,512]{1,0:T(8,128)(2,1)} %param.7), channel_id=1, source_target_pairs={{0,0},{4,1},{8,2},{12,3},{5,4},{1,5},{13,6},{9,7},{10,8},{14,9},{2... | collective-permute-start | bytes 786440 | tf_op jit(solution)/shard_map/ppermute | solution.py:29
  25.3 27.0 %copy-start.3 = (bf16[256,512]{1,0:T(8,128)(2,1)}, bf16[256,512]{1,0:T(8,128)(2,1)S(1)}, u32[]{:S(2)}) copy-start(bf16[256,512]{1,0:T(8,128)(2,1)S(1)} %collective-permute-done) | copy-start | bytes 786436
  25.3 22.3 %collective-permute-start.6 = (bf16[256,512]{1,0:T(8,128)(2,1)S(1)}, bf16[256,512]{1,0:T(8,128)(2,1)S(1)}, u32[]{:S(2)}, u32[]{:S(2)}) collective-permute-start(bf16[256,512]{1,0:T(8,128)(2,1)S(1)} %collective-permute-done), channel_id=1, source_target_pairs={{0,3},{1,2},{2,1},{3,0},{4,7},{5,6},{6,5},{7,4},{8,11},{9,10},{10,... | collective-permute-start | bytes 786440 | tf_op jit(solution)/shard_map/ppermute | solution.py:29
  28.7 39.5 %collective-permute-start.1 = (bf16[256,1024]{1,0:T(8,128)(2,1)}, bf16[256,1024]{1,0:T(8,128)(2,1)}, u32[]{:S(2)}, u32[]{:S(2)}) collective-permute-start(bf16[256,1024]{1,0:T(8,128)(2,1)} %convolution_convert_fusion.3), channel_id=1, source_target_pairs={{0,0},{1,5},{2,10},{3,15},{4,4},{5,1},{6,14},{7,11},{8,8},{9,13},{... | collective-permute-start | bytes 1572872 | tf_op jit(solution)/shard_map/ppermute | solution.py:29
  30.6 20.4 %collective-permute-start.4 = (bf16[256,512]{1,0:T(8,128)(2,1)S(1)}, bf16[256,512]{1,0:T(8,128)(2,1)S(1)}, u32[]{:S(2)}, u32[]{:S(2)}) collective-permute-start(bf16[256,512]{1,0:T(8,128)(2,1)S(1)} %collective-permute-done), channel_id=1, source_target_pairs={{0,2},{1,3},{2,0},{3,1},{4,6},{5,7},{6,4},{7,5},{8,10},{9,11},{10,... | collective-permute-start | bytes 786440 | tf_op jit(solution)/shard_map/ppermute | solution.py:29
  35.3 22.4 %collective-permute-start.2 = (bf16[256,512]{1,0:T(8,128)(2,1)S(1)}, bf16[256,512]{1,0:T(8,128)(2,1)S(1)}, u32[]{:S(2)}, u32[]{:S(2)}) collective-permute-start(bf16[256,512]{1,0:T(8,128)(2,1)S(1)} %collective-permute-done), channel_id=1, source_target_pairs={{0,1},{1,0},{2,3},{3,2},{4,5},{5,4},{6,7},{7,6},{8,9},{9,8},{10,11... | collective-permute-start | bytes 786440 | tf_op jit(solution)/shard_map/ppermute | solution.py:29
  48.9 12.1 %copy-start.1 = (bf16[256,1024]{1,0:T(8,128)(2,1)S(1)}, bf16[256,1024]{1,0:T(8,128)(2,1)}, u32[]{:S(2)}) copy-start(bf16[256,1024]{1,0:T(8,128)(2,1)} %param.9) | copy-start | bytes 1572868
  48.9 13.0 %copy-start = (f32[512,1024]{1,0:T(8,128)S(1)}, f32[512,1024]{1,0:T(8,128)}, u32[]{:S(2)}) copy-start(f32[512,1024]{1,0:T(8,128)} %param.10) | copy-start | bytes 6291460
  48.9 19.4 %collective-permute-start.7 = (bf16[256,1024]{1,0:T(8,128)(2,1)}, bf16[256,1024]{1,0:T(8,128)(2,1)}, u32[]{:S(2)}, u32[]{:S(2)}) collective-permute-start(bf16[256,1024]{1,0:T(8,128)(2,1)} %convolution_convert_fusion), channel_id=1, source_target_pairs={{0,12},{1,9},{2,6},{3,3},{4,8},{5,13},{6,2},{7,7},{8,4},{9,1},{10,... | collective-permute-start | bytes 1572872 | tf_op jit(solution)/shard_map/ppermute | solution.py:29
  51.0 7.9 %copy-start.4 = (bf16[256,512]{1,0:T(8,128)(2,1)}, bf16[256,512]{1,0:T(8,128)(2,1)S(1)}, u32[]{:S(2)}) copy-start(bf16[256,512]{1,0:T(8,128)(2,1)S(1)} %collective-permute-done.4) | copy-start | bytes 786436
  52.3 17.2 %collective-permute-start.5 = (bf16[256,1024]{1,0:T(8,128)(2,1)}, bf16[256,1024]{1,0:T(8,128)(2,1)}, u32[]{:S(2)}, u32[]{:S(2)}) collective-permute-start(bf16[256,1024]{1,0:T(8,128)(2,1)} %convolution_convert_fusion.1), channel_id=1, source_target_pairs={{0,8},{1,13},{2,2},{3,7},{4,12},{5,9},{6,6},{7,3},{8,0},{9,5},{10,... | collective-permute-start | bytes 1572872 | tf_op jit(solution)/shard_map/ppermute | solution.py:29
  57.7 3.2 %copy-start.5 = (bf16[256,512]{1,0:T(8,128)(2,1)}, bf16[256,512]{1,0:T(8,128)(2,1)S(1)}, u32[]{:S(2)}) copy-start(bf16[256,512]{1,0:T(8,128)(2,1)S(1)} %collective-permute-done.2) | copy-start | bytes 786436
  59.0 15.8 %collective-permute-start.3 = (bf16[256,1024]{1,0:T(8,128)(2,1)}, bf16[256,1024]{1,0:T(8,128)(2,1)}, u32[]{:S(2)}, u32[]{:S(2)}) collective-permute-start(bf16[256,1024]{1,0:T(8,128)(2,1)} %convolution_convert_fusion.2), channel_id=1, source_target_pairs={{0,4},{1,1},{2,14},{3,11},{4,0},{5,5},{6,10},{7,15},{8,12},{9,9},{... | collective-permute-start | bytes 1572872 | tf_op jit(solution)/shard_map/ppermute | solution.py:29
  63.0 24.2 %collective-permute-start.21 = (bf16[256,1024]{1,0:T(8,128)(2,1)}, bf16[256,1024]{1,0:T(8,128)(2,1)S(1)}, u32[]{:S(2)}, u32[]{:S(2)}) collective-permute-start(bf16[256,1024]{1,0:T(8,128)(2,1)} %multiply_convert_fusion), channel_id=1, source_target_pairs={{0,8},{4,12},{8,0},{12,4},{1,9},{5,13},{9,1},{13,5},{2,10},{6,14},... | collective-permute-start | bytes 1572872 | tf_op jit(solution)/shard_map/ppermute | solution.py:29
  66.2 10.4 %copy-start.2 = (bf16[256,1024]{1,0:T(8,128)(2,1)S(1)}, bf16[256,1024]{1,0:T(8,128)(2,1)}, u32[]{:S(2)}) copy-start(bf16[256,1024]{1,0:T(8,128)(2,1)} %param.9) | copy-start | bytes 1572868
  66.2 10.4 %copy-start.7 = (f32[1024]{0:T(1024)S(1)}, f32[1024]{0:T(1024)}, u32[]{:S(2)}) copy-start(f32[1024]{0:T(1024)} %param.11) | copy-start | bytes 12292
  68.2 10.8 %collective-permute-start.16 = (bf16[256,512]{1,0:T(8,128)(2,1)}, bf16[256,512]{1,0:T(8,128)(2,1)S(1)}, u32[]{:S(2)}, u32[]{:S(2)}) collective-permute-start(bf16[256,512]{1,0:T(8,128)(2,1)} %collective-permute-done.15), channel_id=1, source_target_pairs={{0,1},{1,0},{2,3},{3,2},{4,5},{5,4},{6,7},{7,6},{8,9},{9,8},{10,11... | collective-permute-start | bytes 786440 | tf_op jit(solution)/shard_map/ppermute | solution.py:29
  68.3 19.0 %collective-permute-start.17 = (bf16[256,512]{1,0:T(8,128)(2,1)}, bf16[256,512]{1,0:T(8,128)(2,1)S(1)}, u32[]{:S(2)}, u32[]{:S(2)}) collective-permute-start(bf16[256,512]{1,0:T(8,128)(2,1)} %collective-permute-done.15), channel_id=1, source_target_pairs={{0,2},{1,3},{2,0},{3,1},{4,6},{5,7},{6,4},{7,5},{8,10},{9,11},{10,... | collective-permute-start | bytes 786440 | tf_op jit(solution)/shard_map/ppermute | solution.py:29
  69.5 25.0 %collective-permute-start.18 = (bf16[256,512]{1,0:T(8,128)(2,1)}, bf16[256,512]{1,0:T(8,128)(2,1)S(1)}, u32[]{:S(2)}, u32[]{:S(2)}) collective-permute-start(bf16[256,512]{1,0:T(8,128)(2,1)} %collective-permute-done.15), channel_id=1, source_target_pairs={{0,3},{1,2},{2,1},{3,0},{4,7},{5,6},{6,5},{7,4},{8,11},{9,10},{10,... | collective-permute-start | bytes 786440 | tf_op jit(solution)/shard_map/ppermute | solution.py:29
  76.6 2.3 %copy-start.6 = (bf16[256,1024]{1,0:T(8,128)(2,1)S(1)}, bf16[256,1024]{1,0:T(8,128)(2,1)}, u32[]{:S(2)}) copy-start(bf16[256,1024]{1,0:T(8,128)(2,1)} %multiply_convert_fusion) | copy-start | bytes 1572868
  76.8 20.9 %collective-permute-start.9 = (bf16[256,1024]{1,0:T(8,128)(2,1)S(1)}, bf16[256,1024]{1,0:T(8,128)(2,1)S(1)}, u32[]{:S(2)}, u32[]{:S(2)}) collective-permute-start(bf16[256,1024]{1,0:T(8,128)(2,1)S(1)} %multiply_convert_fusion.1), channel_id=1, source_target_pairs={{0,8},{4,12},{8,0},{12,4},{1,9},{5,13},{9,1},{13,5},{2,10},{6,14},... | collective-permute-start | bytes 1572872 | tf_op jit(solution)/shard_map/ppermute | solution.py:29
  79.0 18.9 %collective-permute-start.20 = (bf16[256,1024]{1,0:T(8,128)(2,1)S(1)}, bf16[256,1024]{1,0:T(8,128)(2,1)S(1)}, u32[]{:S(2)}, u32[]{:S(2)}) collective-permute-start(bf16[256,1024]{1,0:T(8,128)(2,1)S(1)} %copy-done.6), channel_id=1, source_target_pairs={{0,4},{4,0},{8,12},{12,8},{1,5},{5,1},{9,13},{13,9},{2,6},{6,2},{1... | collective-permute-start | bytes 1572872 | tf_op jit(solution)/shard_map/ppermute | solution.py:29
  87.2 10.7 %collective-permute-start.22 = (bf16[256,1024]{1,0:T(8,128)(2,1)S(1)}, bf16[256,1024]{1,0:T(8,128)(2,1)S(1)}, u32[]{:S(2)}, u32[]{:S(2)}) collective-permute-start(bf16[256,1024]{1,0:T(8,128)(2,1)S(1)} %collective-permute-done.21), channel_id=1, source_target_pairs={{0,4},{4,0},{8,12},{12,8},{1,5},{5,1},{9,13},{13,9},{2,6},{6,2},{1... | collective-permute-start | bytes 1572872 | tf_op jit(solution)/shard_map/ppermute | solution.py:29
  94.6 6.1 %collective-permute-start.8 = (bf16[256,1024]{1,0:T(8,128)(2,1)S(1)}, bf16[256,1024]{1,0:T(8,128)(2,1)S(1)}, u32[]{:S(2)}, u32[]{:S(2)}) collective-permute-start(bf16[256,1024]{1,0:T(8,128)(2,1)S(1)} %multiply_convert_fusion.1), channel_id=1, source_target_pairs={{0,4},{4,0},{8,12},{12,8},{1,5},{5,1},{9,13},{13,9},{2,6},{6,2},{1... | collective-permute-start | bytes 1572872 | tf_op jit(solution)/shard_map/ppermute | solution.py:29
  97.8 3.0 %collective-permute-start.10 = (bf16[256,1024]{1,0:T(8,128)(2,1)S(1)}, bf16[256,1024]{1,0:T(8,128)(2,1)S(1)}, u32[]{:S(2)}, u32[]{:S(2)}) collective-permute-start(bf16[256,1024]{1,0:T(8,128)(2,1)S(1)} %collective-permute-done.9), channel_id=1, source_target_pairs={{0,4},{4,0},{8,12},{12,8},{1,5},{5,1},{9,13},{13,9},{2,6},{6,2},{1... | collective-permute-start | bytes 1572872 | tf_op jit(solution)/shard_map/ppermute | solution.py:29
  99.2 28.8 %collective-permute-start.23 = (bf16[1024,512]{1,0:T(8,128)(2,1)S(1)}, bf16[1024,512]{1,0:T(8,128)(2,1)S(1)}, u32[]{:S(2)}, u32[]{:S(2)}) collective-permute-start(bf16[1024,512]{1,0:T(8,128)(2,1)S(1)} %get-tuple-element.17), channel_id=1, source_target_pairs={{0,16},{16,0},{1,17},{17,1},{2,18},{18,2},{3,19},{19,3},{4,20},{20... | collective-permute-start | bytes 3145736 | tf_op jit(solution)/shard_map/ppermute | solution.py:29
  102.0 45.3 %collective-permute-start.19 = (bf16[512,1024]{1,0:T(8,128)(2,1)S(1)}, bf16[512,1024]{1,0:T(8,128)(2,1)S(1)}, u32[]{:S(2)}, u32[]{:S(2)}) collective-permute-start(bf16[512,1024]{1,0:T(8,128)(2,1)S(1)} %get-tuple-element.15), channel_id=1, source_target_pairs={{0,16},{16,0},{1,17},{17,1},{2,18},{18,2},{3,19},{19,3},{4,20},{20... | collective-permute-start | bytes 3145736 | tf_op jit(solution)/shard_map/ppermute | solution.py:29
  104.3 18.6 %collective-permute-start.13 = (bf16[256,512]{1,0:T(8,128)(2,1)S(1)}, bf16[256,512]{1,0:T(8,128)(2,1)S(1)}, u32[]{:S(2)}, u32[]{:S(2)}) collective-permute-start(bf16[256,512]{1,0:T(8,128)(2,1)S(1)} %convolution_convert_fusion.4), channel_id=1, source_target_pairs={{0,3},{1,2},{2,1},{3,0},{4,7},{5,6},{6,5},{7,4},{8,11},{9,10},{10,... | collective-permute-start | bytes 786440 | tf_op jit(solution)/shard_map/ppermute | solution.py:29
  104.5 20.8 %collective-permute-start.12 = (bf16[256,512]{1,0:T(8,128)(2,1)S(1)}, bf16[256,512]{1,0:T(8,128)(2,1)S(1)}, u32[]{:S(2)}, u32[]{:S(2)}) collective-permute-start(bf16[256,512]{1,0:T(8,128)(2,1)S(1)} %convolution_convert_fusion.5), channel_id=1, source_target_pairs={{0,2},{1,3},{2,0},{3,1},{4,6},{5,7},{6,4},{7,5},{8,10},{9,11},{10,... | collective-permute-start | bytes 786440 | tf_op jit(solution)/shard_map/ppermute | solution.py:29
  105.4 19.9 %collective-permute-start.11 = (bf16[256,512]{1,0:T(8,128)(2,1)S(1)}, bf16[256,512]{1,0:T(8,128)(2,1)S(1)}, u32[]{:S(2)}, u32[]{:S(2)}) collective-permute-start(bf16[256,512]{1,0:T(8,128)(2,1)S(1)} %convolution_convert_fusion.6), channel_id=1, source_target_pairs={{0,1},{1,0},{2,3},{3,2},{4,5},{5,4},{6,7},{7,6},{8,9},{9,8},{10,11... | collective-permute-start | bytes 786440 | tf_op jit(solution)/shard_map/ppermute | solution.py:29
  125.8 10.0 %collective-permute-start.14 = (bf16[256,512]{1,0:T(8,128)(2,1)S(1)}, bf16[256,512]{1,0:T(8,128)(2,1)S(1)}, u32[]{:S(2)}, u32[]{:S(2)}) collective-permute-start(bf16[256,512]{1,0:T(8,128)(2,1)S(1)} %fusion.12), channel_id=1, source_target_pairs={{0,0},{1,4},{2,8},{3,12},{4,5},{5,1},{6,13},{7,9},{8,10},{9,14},{1... | collective-permute-start | bytes 786440 | tf_op jit(solution)/shard_map/ppermute | solution.py:29
